TPU v7x, 256 devices: a 4x2x16 block of a 4x16x16 slice. The times are simulated.
256 devices in a mesh: grp: 2 (over y), sp: 16 (over z), tp: 8 (over x, core).
Axes of the slice: x: 4, y: 2, z: 16, core: 2. Of those that a mesh axis runs over, the one named last changes fastest.
The devices are a block of a 4x16x16 slice.
Arguments:
- tokens: bfloat16 [32, 4096, 4096], P(('grp', 'tp'), 'sp'), parts along dimension 0, may hold values from -8 to 8, as said below
- offsets: int32 [32], P(('grp', 'tp')), parts along dimension 0, may hold values from 0 to 4095
- in_gain: float32 [4096], replicated, may hold values from 0.1 to 1.9
- w_latent: bfloat16 [4096, 1024], P('sp'), may hold values from -0.09375 to 0.09375
- w_rope_key: bfloat16 [4096, 32], replicated, may hold values from -0.09375 to 0.09375
- kv_gain: float32 [1024], replicated, may hold values from 0.1 to 1.9
- w_up_key: bfloat16 [1024, 2048], P(None, 'tp'), may hold values from -0.1875 to 0.1875
- w_up_value: bfloat16 [1024, 2048], P(None, 'tp'), may hold values from -0.1875 to 0.1875
- q_nope: bfloat16 [32, 2048], P(('grp', 'sp'), 'tp'), parts along dimension 0, may hold values from -300 to 300, as said below
- q_rope: bfloat16 [32, 1024], P(('grp', 'sp'), 'tp'), parts along dimension 0, may hold values from -16 to 16
Outputs:
- keys: bfloat16 [32, 4096, 2048], P(('grp', 'sp'), None, 'tp'), parts along dimension 0
- values: bfloat16 [32, 4096, 2048], P(('grp', 'sp'), None, 'tp'), parts along dimension 0
- rope_keys: bfloat16 [32, 32, 4096], P(('grp', 'sp')), parts along dimension 0
- read: bfloat16 [32, 2048], P(('grp', 'sp'), 'tp'), parts along dimension 0
There are 2 independent parts, one for each index of `grp`. A program takes and returns all parts, laid end to end along the dimension named above; an argument that names none is the same for every part. Nothing has to cross between parts.
Inputs may be any that keep to these rules, and one draw needn't show every extreme that they name: `tokens`: entries of the layer's input. `q_nope`: entries of the first decoding token's queries.
All inputs are finite; a program needn't handle non-finite values.
Results may differ from a plain program's by a relative error of at most 0.02.
Values may be sent and summed in bfloat16 or wider, within the bound.
A program may use at most 128 MiB of HBM per device.

v0:
```python
import jax
import jax.numpy as jnp
from jax import lax
from jax.sharding import PartitionSpec as P

HEAD = 64
ROPE = 32
EPS = 1e-06


def joined_along(tiles, dim):
    shape = list(tiles.shape[1:])
    shape[dim] *= tiles.shape[0]
    return jnp.moveaxis(tiles, 0, dim).reshape(shape)


def copy_for_each(value, axis):
    peers = lax.axis_size(axis)
    return lax.all_to_all(
        jnp.broadcast_to(value[None], (peers, *value.shape)), axis, 0, 0, tiled=True
    )


def gather_directly(value, axis, dim):
    return joined_along(copy_for_each(value, axis), dim)


def rms_scale(values, gain):
    wide = values.astype(jnp.float32)
    return wide * lax.rsqrt(jnp.mean(wide * wide, axis=-1, keepdims=True) + EPS) * gain


def rotate(raw, position):
    inverse = 10000.0 ** (-jnp.arange(0, ROPE, 2).astype(jnp.float32) / ROPE)
    angle = position.astype(jnp.float32)[..., None] * inverse
    cosine, sine = (jnp.cos(angle), jnp.sin(angle))
    half = ROPE // 2
    first, second = (raw[..., :half], raw[..., half:])
    return jnp.concatenate(
        [first * cosine - second * sine, second * cosine + first * sine], axis=-1
    )


def local(
    tokens, offsets, in_gain, w_latent, w_rope_key, kv_gain, w_up_key, w_up_value, q_nope, q_rope
):
    prompts, rows, width = tokens.shape
    n_sp = lax.axis_size("sp")
    length = n_sp * rows
    block = lax.axis_index("sp")
    normed = rms_scale(tokens.reshape(prompts * rows, width), in_gain).astype(jnp.bfloat16)
    latent_raw = jnp.dot(
        normed,
        lax.all_gather(w_latent, "sp", axis=0, tiled=True),
        preferred_element_type=jnp.float32,
    )
    latent = rms_scale(latent_raw, kv_gain).astype(jnp.bfloat16)
    position = offsets[:, None] + block * rows + jnp.arange(rows, dtype=jnp.int32)[None, :]
    rope_raw = jnp.dot(normed, w_rope_key, preferred_element_type=jnp.float32).reshape(
        prompts, rows, ROPE
    )
    rotated = rotate(rope_raw, position).astype(jnp.bfloat16)
    head_cols = w_up_key.shape[1]
    paired = jnp.stack([w_up_key, w_up_value])
    both = jnp.einsum(
        "tk,skc->stc",
        latent,
        lax.all_gather(paired, "tp", axis=2, tiled=True),
        preferred_element_type=jnp.float32,
    ).astype(jnp.bfloat16)
    both = both.reshape(2, prompts, rows, both.shape[2])
    by_head = lax.all_to_all(both, "tp", split_axis=3, concat_axis=1, tiled=True)
    rope_every = gather_directly(rotated, "tp", 0)
    moved, rope_moved = (
        lax.all_to_all(by_head[:, :, None], "sp", split_axis=1, concat_axis=2, tiled=True),
        lax.all_to_all(rope_every[None, :, None], "sp", split_axis=1, concat_axis=2, tiled=True),
    )
    keys = moved[0].reshape(length, head_cols)
    values = moved[1].reshape(length, head_cols)
    rope_all = rope_moved.reshape(length, ROPE)
    rope_keys = rope_all.T
    heads_here = head_cols // HEAD
    query = q_nope.reshape(heads_here, HEAD)
    rotary_q = q_rope.reshape(heads_here, ROPE)
    keys_split = keys.reshape(length, heads_here, HEAD)
    scores = jnp.einsum("hd,jhd->hj", query, keys_split, preferred_element_type=jnp.float32)
    scores = scores + jnp.dot(rotary_q, rope_keys, preferred_element_type=jnp.float32)
    scores = scores / jnp.sqrt(jnp.float32(HEAD + ROPE))
    peak = jnp.max(scores, axis=-1, keepdims=True)
    expo = jnp.exp(scores - peak)
    weights = (expo / jnp.sum(expo, axis=-1, keepdims=True)).astype(jnp.bfloat16)
    read = jnp.einsum(
        "hj,jhd->hd",
        weights,
        values.reshape(length, heads_here, HEAD),
        preferred_element_type=jnp.float32,
    )
    read = read.astype(jnp.bfloat16).reshape(1, heads_here * HEAD)
    return (keys[None], values[None], rope_keys[None], read)


def solution(mesh):
    in_specs = (
        P(("grp", "tp"), "sp", None),
        P(("grp", "tp")),
        P(),
        P("sp", None),
        P(),
        P(),
        P(None, "tp"),
        P(None, "tp"),
        P(("grp", "sp"), "tp"),
        P(("grp", "sp"), "tp"),
    )
    out_specs = (
        P(("grp", "sp"), None, "tp"),
        P(("grp", "sp"), None, "tp"),
        P(("grp", "sp"), None, None),
        P(("grp", "sp"), "tp"),
    )
    return jax.shard_map(local, mesh=mesh, in_specs=in_specs, out_specs=out_specs, check_vma=False)
```

profile of v0, /device:TPU:33, one launch (start us, length us, event | category | flops | bytes accessed | tf_op | source)
XLA Modules:
  0.0 515.6 jit_solution(11231751343885072324)
XLA Ops:
  7.2 0.0 copy-start
  7.2 0.0 copy-start.6
  7.2 0.1 all-gather.5.cloned.1.call-start
  7.3 0.7 all-gather.5.cloned.1.call-update
  8.0 0.1 all-gather.3.cloned.1.call-start
  8.1 2.3 pad_maximum_fusion
  10.3 0.1 all-gather.3.cloned.1.call-update
  10.4 0.0 copy-start.3
  10.4 0.8 broadcast_add_fusion
  11.2 0.1 add_convert_fusion
  11.3 3.3 multiply_reduce_fusion
  14.6 0.0 copy-done
  14.6 0.0 copy-done.6
  14.6 0.0 copy-done.3
  14.7 1.4 fusion.4
  16.1 0.2 fusion.21
  16.4 0.8 broadcast_in_dim.7
  17.2 23.7 %all-to-all-start.2 = ((bf16[8,2,256,32]{2,1,3,0:T(2,128)(2,1)}), bf16[8,2,256,32]{2,1,3,0:T(2,128)(2,1)S(1)}, u32[]{:S(2)}, u32[]{:S(2)}) async-start(bf16[8,2,256,32]{2,1,3,0:T(2,128)(2,1)} %broadcast_in_dim.7), calls=%async_computation.2 | async-start | bytes 524288 | tf_op jit(solution)/shard_map/all_to_all | solution.py:19
  40.9 5.8 %fusion.1 = bf16[512,4096]{1,0:T(8,128)(2,1)} fusion(bf16[2,256,4096]{2,1,0:T(8,128)(2,1)} %param.10, f32[4096]{0:T(1024)S(1)} %copy-done.6, f32[512]{0:T(512)S(1)} %bitcast.76), kind=kLoop, calls=%fused_computation.2 | loop fusion | flops 8388608 | bytes 8407040 | tf_op jit(solution)/shard_map/convert_element_type | solution.py:51
  46.7 0.0 copy-start.8
  46.7 81.6 %all-gather.5.cloned.1.call-done = bf16[4096,1024]{1,0:T(8,128)(2,1)} async-done(((bf16[256,1024]{1,0:T(8,128)(2,1)}), bf16[4096,1024]{1,0:T(8,128)(2,1)}) %all-gather.5.cloned.1.call-update) | async-done | bytes 8388624 | tf_op jit(solution)/shard_map/all_gather | solution.py:54
  128.3 8.3 %multiply_reduce_fusion.1 = (f32[512]{0:T(512)S(1)}, f32[512,1024]{1,0:T(8,128)S(1)}) fusion(bf16[512,4096]{1,0:T(8,128)(2,1)} %fusion.1, bf16[4096,1024]{1,0:T(8,128)(2,1)} %all-gather.5.cloned.1.call-done), kind=kOutput, calls=%fused_computation.14 | convolution fusion | flops 4296015360 | bytes 14682112 | tf_op jit(solution)/shard_map/dot_general | solution.py:52
  136.6 52.3 %all-gather.3.cloned.1.call-done = bf16[2,1024,2048]{2,1,0:T(8,128)(2,1)} async-done(((bf16[2,1024,256]{2,1,0:T(8,128)(2,1)}), bf16[2,1024,2048]{2,1,0:T(8,128)(2,1)}) %all-gather.3.cloned.1.call-update) | async-done | bytes 8388624 | tf_op jit(solution)/shard_map/all_gather | solution.py:68
  188.9 0.0 copy-done.8
  188.9 9.6 %convolution_convert_fusion = bf16[2,2048,512]{1,2,0:T(8,128)(2,1)} fusion(bf16[2,1024,2048]{2,1,0:T(8,128)(2,1)} %all-gather.3.cloned.1.call-done, f32[512,1024]{1,0:T(8,128)S(1)} %get-tuple-element.11, f32[1024]{0:T(1024)S(1)} %copy-done.8, f32[512]{0:T(512)S(1)} %add_rsqrt_fusion), kind=kOutput, calls=%fused_computation.12 | convolution fusion | flops 4298637312 | bytes 14686208 | tf_op jit(solution)/shard_map/tk,skc->stc/dot_general | solution.py:65
  198.6 11.2 %copy.25 = bf16[2,2,256,2048]{2,1,0,3:T(2,128)(2,1)} copy(bf16[2,2,256,2048]{3,2,1,0:T(8,128)(2,1)} %bitcast.68) | data formatting | bytes 8388608 | tf_op jit(solution)/shard_map/reshape | solution.py:71
  209.8 0.0 all-to-all-done.2
  209.8 4.7 all-to-all-start
  214.4 0.7 copy.30
  215.2 48.1 %all-to-all-done = bf16[2,2,256,2048]{2,1,0,3:T(2,128)(2,1)} async-done(((bf16[2,2,256,2048]{2,1,0,3:T(2,128)(2,1)}), bf16[2,2,256,2048]{2,1,0,3:T(2,128)(2,1)}, u32[]{:S(2)}, u32[]{:S(2)}) %all-to-all-start) | async-done | bytes 4194336 | tf_op jit(solution)/shard_map/all_to_all | solution.py:72
  263.3 12.1 %all-to-all-start.3 = ((bf16[1,16,1,256,32]{3,4,2,0,1:T(8,128)(2,1)}), bf16[1,16,1,256,32]{3,4,2,0,1:T(8,128)(2,1)S(1)}, u32[]{:S(2)}, u32[]{:S(2)}) async-start(bf16[1,16,1,256,32]{3,4,2,0,1:T(8,128)(2,1)} %bitcast.13), calls=%async_computation.3 | async-start | bytes 524288 | tf_op jit(solution)/shard_map/all_to_all | solution.py:76
  275.4 4.9 copy.26
  280.4 7.7 %all-to-all-done.3 = bf16[1,16,1,256,32]{3,4,2,0,1:T(8,128)(2,1)S(1)} async-done(((bf16[1,16,1,256,32]{3,4,2,0,1:T(8,128)(2,1)}), bf16[1,16,1,256,32]{3,4,2,0,1:T(8,128)(2,1)S(1)}, u32[]{:S(2)}, u32[]{:S(2)}) %all-to-all-start.3) | async-done | bytes 262176 | tf_op jit(solution)/shard_map/all_to_all | solution.py:76
  288.1 0.0 copy-start.7
  288.1 0.0 copy-start.9
  288.1 11.6 %all-to-all-start.1 = ((bf16[2,16,1,256,256]{3,4,2,0,1:T(8,128)(2,1)}), bf16[2,16,1,256,256]{3,4,2,0,1:T(8,128)(2,1)}, u32[]{:S(2)}, u32[]{:S(2)}) async-start(bf16[2,16,1,256,256]{3,4,2,0,1:T(8,128)(2,1)} %bitcast.67), calls=%async_computation.1 | async-start | bytes 8388608 | tf_op jit(solution)/shard_map/all_to_all | solution.py:75
  299.7 0.0 copy-done.7
  299.7 0.1 reshape.142
  299.8 0.5 broadcast.98
  300.3 0.0 copy-done.9
  300.3 0.7 reduce.5
  301.0 0.1 reshape.132
  301.1 0.0 copy-start.5
  301.1 180.2 %all-to-all-done.1 = bf16[2,16,1,256,256]{3,4,2,0,1:T(8,128)(2,1)} async-done(((bf16[2,16,1,256,256]{3,4,2,0,1:T(8,128)(2,1)}), bf16[2,16,1,256,256]{3,4,2,0,1:T(8,128)(2,1)}, u32[]{:S(2)}, u32[]{:S(2)}) %all-to-all-start.1) | async-done | bytes 4194336 | tf_op jit(solution)/shard_map/all_to_all | solution.py:75
  481.3 2.6 fusion.26
  483.9 0.0 copy-start.2
  483.9 1.3 copy-done.2
  485.2 2.5 copy.34
  487.8 3.9 copy.40
  491.7 2.5 copy.33
  494.2 2.4 copy.39
  496.5 0.0 copy-start.4
  496.5 0.0 copy-start.1
  496.5 4.3 reshape_reshape_squeeze.6
  500.9 2.0 fusion.28
  502.8 0.0 copy-done.5
  502.8 0.3 fusion.27
  503.1 0.2 fusion.15
  503.3 0.1 fusion.24
  503.5 0.0 copy-done.4
  503.5 2.3 reshape_reshape_squeeze.7
  505.8 2.2 fusion.13
  508.0 0.7 reshape.133
  508.7 0.0 copy-done.1
  (9 shorter events, 0.1 us)
Async XLA Ops:
  7.2 7.4 %copy-start = (bf16[4096,32]{0,1:T(8,128)(2,1)S(1)}, bf16[4096,32]{0,1:T(8,128)(2,1)}, u32[]{:S(2)}) copy-start(bf16[4096,32]{0,1:T(8,128)(2,1)} %param.14) | copy-start | bytes 786436
  7.2 7.4 %copy-start.6 = (f32[4096]{0:T(1024)S(1)}, f32[4096]{0:T(1024)}, u32[]{:S(2)}) copy-start(f32[4096]{0:T(1024)} %param.12) | copy-start | bytes 49156
  7.2 121.1 %all-gather.5.cloned.1.call-start = ((), (), s32[]{:S(2)}) async-start(), calls=%async_computation.5 | async-start | bytes 8912896 | tf_op jit(solution)/shard_map/all_gather | solution.py:54
  8.0 180.9 %all-gather.3.cloned.1.call-start = ((), (), s32[]{:S(2)}) async-start(), calls=%async_computation.4 | async-start | bytes 9437184 | tf_op jit(solution)/shard_map/all_gather | solution.py:68
  10.4 4.2 copy-start.3
  17.2 192.6 %all-to-all-start.2 = ((bf16[8,2,256,32]{2,1,3,0:T(2,128)(2,1)}), bf16[8,2,256,32]{2,1,3,0:T(2,128)(2,1)S(1)}, u32[]{:S(2)}, u32[]{:S(2)}) async-start(bf16[8,2,256,32]{2,1,3,0:T(2,128)(2,1)} %broadcast_in_dim.7), calls=%async_computation.2 | async-start | bytes 524288 | tf_op jit(solution)/shard_map/all_to_all | solution.py:19
  46.7 142.2 %copy-start.8 = (f32[1024]{0:T(1024)S(1)}, f32[1024]{0:T(1024)}, u32[]{:S(2)}) copy-start(f32[1024]{0:T(1024)} %param.15) | copy-start | bytes 12292
  209.8 53.6 %all-to-all-start = ((bf16[2,2,256,2048]{2,1,0,3:T(2,128)(2,1)}), bf16[2,2,256,2048]{2,1,0,3:T(2,128)(2,1)}, u32[]{:S(2)}, u32[]{:S(2)}) async-start(bf16[2,2,256,2048]{2,1,0,3:T(2,128)(2,1)} %copy.25), calls=%async_computation | async-start | bytes 8388608 | tf_op jit(solution)/shard_map/all_to_all | solution.py:72
  263.3 24.8 %all-to-all-start.3 = ((bf16[1,16,1,256,32]{3,4,2,0,1:T(8,128)(2,1)}), bf16[1,16,1,256,32]{3,4,2,0,1:T(8,128)(2,1)S(1)}, u32[]{:S(2)}, u32[]{:S(2)}) async-start(bf16[1,16,1,256,32]{3,4,2,0,1:T(8,128)(2,1)} %bitcast.13), calls=%async_computation.3 | async-start | bytes 524288 | tf_op jit(solution)/shard_map/all_to_all | solution.py:76
  288.1 11.6 %copy-start.7 = (bf16[1,256]{1,0:T(2,128)(2,1)S(1)}, bf16[1,256]{1,0:T(2,128)(2,1)}, u32[]{:S(2)}) copy-start(bf16[1,256]{1,0:T(2,128)(2,1)} %param.18) | copy-start | bytes 1540
  288.1 12.2 %copy-start.9 = (bf16[1,128]{1,0:T(2,128)(2,1)S(1)}, bf16[1,128]{1,0:T(2,128)(2,1)}, u32[]{:S(2)}) copy-start(bf16[1,128]{1,0:T(2,128)(2,1)} %param.19) | copy-start | bytes 772
  288.1 193.2 %all-to-all-start.1 = ((bf16[2,16,1,256,256]{3,4,2,0,1:T(8,128)(2,1)}), bf16[2,16,1,256,256]{3,4,2,0,1:T(8,128)(2,1)}, u32[]{:S(2)}, u32[]{:S(2)}) async-start(bf16[2,16,1,256,256]{3,4,2,0,1:T(8,128)(2,1)} %bitcast.67), calls=%async_computation.1 | async-start | bytes 8388608 | tf_op jit(solution)/shard_map/all_to_all | solution.py:75
  301.1 201.8 %copy-start.5 = (bf16[4,8,16,256]{3,1,2,0:T(8,128)(2,1)}, bf16[4,8,16,256]{3,1,2,0:T(8,128)(2,1)S(1)}, u32[]{:S(2)}) copy-start(bf16[4,8,16,256]{3,1,2,0:T(8,128)(2,1)S(1)} %copy.44) | copy-start | bytes 786436
  483.9 1.3 copy-start.2
  496.5 6.9 %copy-start.4 = (bf16[1,16,1,256,256]{3,1,4,2,0:T(8,128)(2,1)S(1)}, bf16[1,16,1,256,256]{3,1,4,2,0:T(8,128)(2,1)}, u32[]{:S(2)}) copy-start(bf16[1,16,1,256,256]{3,1,4,2,0:T(8,128)(2,1)} %copy.34) | copy-start | bytes 6291460
  496.5 12.2 %copy-start.1 = (bf16[4096,32]{0,1:T(8,128)(2,1)S(1)}, bf16[4096,32]{0,1:T(8,128)(2,1)}, u32[]{:S(2)}) copy-start(bf16[4096,32]{0,1:T(8,128)(2,1)} %param.14) | copy-start | bytes 786436
Sparse Core Ops, SparseCore 0:
  9.8 118.4 all-gather.4
  130.7 58.1 all-gather.2
where the time goes:
time: 517 us; the launch traced here: 516 us
  waiting for transfers between devices  371 us (72%)
  starting transfers between devices  52.2 us (10%)
  local copies, waits for them, and re-layouts  41 us (8%)
  matrix products  23.8 us (5%)
  between operations  14.2 us (3%)
  other arithmetic  13.5 us (3%)
    all_to_all x1, waiting for transfers between devices, local(): lax.all_to_all(by_head[:, :, None], 'sp', split_axis=1, concat_axis=2, ti...  180 us
    all_gather x1, waiting for transfers between devices, local(): lax.all_gather(w_latent, 'sp', axis=0, tiled=True)  81.6 us
    all_gather x1, waiting for transfers between devices, local(): lax.all_gather(paired, 'tp', axis=2, tiled=True)  52.3 us
    all_to_all x1, waiting for transfers between devices, local(): lax.all_to_all(both, 'tp', split_axis=3, concat_axis=1, tiled=True)  48.1 us
    all_to_all x1, starting transfers between devices, copy_for_each(): lax.all_to_all(jnp.broadcast_to(value[None], (peers, *value.shape)), axis...  23.7 us
    all_to_all x1, starting transfers between devices, local(): lax.all_to_all(rope_every[None, :, None], 'sp', split_axis=1, concat_axis...  12.1 us
    all_to_all x1, starting transfers between devices, local(): lax.all_to_all(by_head[:, :, None], 'sp', split_axis=1, concat_axis=2, ti...  11.6 us
    reshape x1, local copies, waits for them, and re-layouts, local(): both = both.reshape(2, prompts, rows, both.shape[2])  11.2 us
  transfers between devices with their start and end apart: 6, of which 5 were waited for; matrix products, arithmetic and copies ran while one was open for 10% of the time, Pallas kernels for 0%

commit v1 on v0

--- a/solution.py
+++ b/solution.py
@@ -69,7 +69,9 @@
         preferred_element_type=jnp.float32,
     ).astype(jnp.bfloat16)
     both = both.reshape(2, prompts, rows, both.shape[2])
-    by_head = lax.all_to_all(both, "tp", split_axis=3, concat_axis=1, tiled=True)
+    parts = jnp.split(both, lax.axis_size("tp"), axis=3)
+    received = lax.all_to_all(jnp.stack(parts), "tp", 0, 0)
+    by_head = jnp.concatenate(received, axis=1)
     rope_every = gather_directly(rotated, "tp", 0)
     moved, rope_moved = (
         lax.all_to_all(by_head[:, :, None], "sp", split_axis=1, concat_axis=2, tiled=True),

time: 517 us -> 504 us (0.975)
  local copies, waits for them, and re-layouts: 41 us -> 31.8 us
    reshape x1 -> x0, local copies, waits for them, and re-layouts: 11.2 us -> none  [local(): both = both.reshape(2, prompts, rows, both.shape[2])]
  transfers between devices with their start and end apart: 6 -> 6, of which waited for: 5 -> 5; matrix products, arithmetic and copies ran while one was open for 10% -> 9% of each run, Pallas kernels for 0% -> 0%
where the time goes in v1:
time: 504 us
  waiting for transfers between devices  371 us (74%)
  starting transfers between devices  52.1 us (10%)
  local copies, waits for them, and re-layouts  31.8 us (6%)
  matrix products  20.9 us (4%)
  between operations  14.3 us (3%)
  other arithmetic  13.5 us (3%)
    all_to_all x1, waiting for transfers between devices, local(): lax.all_to_all(by_head[:, :, None], 'sp', split_axis=1, concat_axis=2, ti...  180 us
    all_gather x1, waiting for transfers between devices, local(): lax.all_gather(w_latent, 'sp', axis=0, tiled=True)  81.6 us
    all_gather x1, waiting for transfers between devices, local(): lax.all_gather(paired, 'tp', axis=2, tiled=True)  52.3 us
    all_to_all x1, waiting for transfers between devices, local(): received = lax.all_to_all(jnp.stack(parts), 'tp', 0, 0)  48.1 us
    all_to_all x1, starting transfers between devices, copy_for_each(): lax.all_to_all(jnp.broadcast_to(value[None], (peers, *value.shape)), axis...  23.7 us
    all_to_all x1, starting transfers between devices, local(): lax.all_to_all(rope_every[None, :, None], 'sp', split_axis=1, concat_axis...  12.1 us
    all_to_all x1, starting transfers between devices, local(): lax.all_to_all(by_head[:, :, None], 'sp', split_axis=1, concat_axis=2, ti...  11.4 us
  transfers between devices with their start and end apart: 6, of which 5 were waited for; matrix products, arithmetic and copies ran while one was open for 9% of the time, Pallas kernels for 0%

profile of v1, /device:TPU:33, one launch (start us, length us, event | category | flops | bytes accessed | tf_op | source)
XLA Modules:
  0.0 503.5 jit_solution(15954407040946968766)
XLA Ops:
  7.2 0.0 copy-start
  7.2 0.0 copy-start.5
  7.2 0.1 all-gather.5.cloned.1.call-start
  7.3 0.7 all-gather.5.cloned.1.call-update
  8.0 0.1 all-gather.3.cloned.1.call-start
  8.1 2.3 pad_maximum_fusion
  10.3 0.1 all-gather.3.cloned.1.call-update
  10.4 0.0 copy-start.2
  10.4 0.8 broadcast_add_fusion
  11.2 0.1 add_convert_fusion
  11.3 3.3 multiply_reduce_fusion
  14.6 0.0 copy-done
  14.6 0.0 copy-done.5
  14.6 0.0 copy-done.2
  14.7 1.4 fusion.4
  16.1 0.2 fusion.29
  16.4 0.8 broadcast_in_dim.4
  17.2 23.7 %all-to-all-start.2 = ((bf16[8,2,256,32]{2,1,3,0:T(2,128)(2,1)}), bf16[8,2,256,32]{2,1,3,0:T(2,128)(2,1)S(1)}, u32[]{:S(2)}, u32[]{:S(2)}) async-start(bf16[8,2,256,32]{2,1,3,0:T(2,128)(2,1)} %broadcast_in_dim.4), calls=%async_computation.2 | async-start | bytes 524288 | tf_op jit(solution)/shard_map/all_to_all | solution.py:19
  40.9 5.8 %fusion.1 = bf16[512,4096]{1,0:T(8,128)(2,1)} fusion(bf16[2,256,4096]{2,1,0:T(8,128)(2,1)} %param.10, f32[4096]{0:T(1024)S(1)} %copy-done.5, f32[512]{0:T(512)S(1)} %bitcast.114), kind=kLoop, calls=%fused_computation.2 | loop fusion | flops 8388608 | bytes 8407040 | tf_op jit(solution)/shard_map/convert_element_type | solution.py:51
  46.7 81.6 %all-gather.5.cloned.1.call-done = bf16[4096,1024]{1,0:T(8,128)(2,1)} async-done(((bf16[256,1024]{1,0:T(8,128)(2,1)}), bf16[4096,1024]{1,0:T(8,128)(2,1)}) %all-gather.5.cloned.1.call-update) | async-done | bytes 8388624 | tf_op jit(solution)/shard_map/all_gather | solution.py:54
  128.3 8.3 %multiply_reduce_fusion.1 = (f32[512]{0:T(512)S(1)}, f32[512,1024]{1,0:T(8,128)S(1)}) fusion(bf16[512,4096]{1,0:T(8,128)(2,1)} %fusion.1, bf16[4096,1024]{1,0:T(8,128)(2,1)} %all-gather.5.cloned.1.call-done), kind=kOutput, calls=%fused_computation.14 | convolution fusion | flops 4296015360 | bytes 14682112 | tf_op jit(solution)/shard_map/dot_general | solution.py:52
  136.6 52.3 %all-gather.3.cloned.1.call-done = bf16[2,1024,2048]{2,1,0:T(8,128)(2,1)} async-done(((bf16[2,1024,256]{2,1,0:T(8,128)(2,1)}), bf16[2,1024,2048]{2,1,0:T(8,128)(2,1)}) %all-gather.3.cloned.1.call-update) | async-done | bytes 8388624 | tf_op jit(solution)/shard_map/all_gather | solution.py:68
  188.9 0.0 copy-done.7
  188.9 8.3 %convolution_convert_fusion = bf16[2,2048,512]{1,2,0:T(8,128)(2,1)S(1)} fusion(bf16[2,1024,2048]{2,1,0:T(8,128)(2,1)} %all-gather.3.cloned.1.call-done, f32[512,1024]{1,0:T(8,128)S(1)} %get-tuple-element.11, f32[1024]{0:T(1024)S(1)} %copy-done.7, f32[512]{0:T(512)S(1)} %add_rsqrt_fusion), kind=kOutput, calls=%fused_computation.12 | convolution fusion | flops 4298637312 | bytes 14686208 | tf_op jit(solution)/shard_map/tk,skc->stc/dot_general | solution.py:65
  197.3 0.9 fusion.19
  198.1 0.9 fusion.18
  199.0 0.9 fusion.17
  199.9 0.9 fusion.16
  200.8 0.9 fusion.15
  201.7 0.9 fusion.14
  202.5 0.9 fusion.13
  203.4 0.9 fusion.12
  204.3 0.0 all-to-all-done.2
  204.4 4.7 all-to-all-start
  209.0 0.7 copy.33
  209.8 48.1 %all-to-all-done = bf16[8,2,2,256,256]{4,3,2,1,0:T(8,128)(2,1)} async-done(((bf16[8,2,2,256,256]{4,3,2,1,0:T(8,128)(2,1)}), bf16[8,2,2,256,256]{4,3,2,1,0:T(8,128)(2,1)}, u32[]{:S(2)}, u32[]{:S(2)}) %all-to-all-start) | async-done | bytes 4194336 | tf_op jit(solution)/shard_map/all_to_all | solution.py:73
  257.9 12.1 %all-to-all-start.3 = ((bf16[1,16,1,256,32]{3,4,2,0,1:T(8,128)(2,1)}), bf16[1,16,1,256,32]{3,4,2,0,1:T(8,128)(2,1)S(1)}, u32[]{:S(2)}, u32[]{:S(2)}) async-start(bf16[1,16,1,256,32]{3,4,2,0,1:T(8,128)(2,1)} %bitcast.21), calls=%async_computation.3 | async-start | bytes 524288 | tf_op jit(solution)/shard_map/all_to_all | solution.py:78
  270.0 2.5 copy.30
  272.5 2.2 copy.31
  274.7 8.0 %all-to-all-done.3 = bf16[1,16,1,256,32]{3,4,2,0,1:T(8,128)(2,1)S(1)} async-done(((bf16[1,16,1,256,32]{3,4,2,0,1:T(8,128)(2,1)}), bf16[1,16,1,256,32]{3,4,2,0,1:T(8,128)(2,1)S(1)}, u32[]{:S(2)}, u32[]{:S(2)}) %all-to-all-start.3) | async-done | bytes 262176 | tf_op jit(solution)/shard_map/all_to_all | solution.py:78
  282.7 11.4 %all-to-all-start.1 = ((bf16[2,16,1,256,256]{4,3,0,2,1:T(8,128)(2,1)}), bf16[2,16,1,256,256]{4,3,0,2,1:T(8,128)(2,1)}, u32[]{:S(2)}, u32[]{:S(2)}) async-start(bf16[2,16,1,256,256]{4,3,0,2,1:T(8,128)(2,1)} %copy.31), calls=%async_computation.1 | async-start | bytes 8388608 | tf_op jit(solution)/shard_map/all_to_all | solution.py:77
  294.1 0.0 copy-done.6
  294.2 0.1 reshape.145
  294.3 0.5 broadcast.98
  294.8 0.0 copy-done.8
  294.8 0.7 reduce.5
  295.4 0.1 reshape.135
  295.6 0.0 copy-start.4
  295.6 180.2 %all-to-all-done.1 = bf16[2,16,1,256,256]{4,3,0,2,1:T(8,128)(2,1)} async-done(((bf16[2,16,1,256,256]{4,3,0,2,1:T(8,128)(2,1)}), bf16[2,16,1,256,256]{4,3,0,2,1:T(8,128)(2,1)}, u32[]{:S(2)}, u32[]{:S(2)}) %all-to-all-start.1) | async-done | bytes 4194336 | tf_op jit(solution)/shard_map/all_to_all | solution.py:77
  475.8 3.9 fusion.34
  479.7 1.3 copy-done.3
  481.0 3.1 copy.36
  484.1 2.9 reshape_reshape_squeeze.6
  487.0 0.4 fusion.36
  487.4 0.0 copy-done.4
  487.4 0.3 fusion.35
  487.7 0.2 fusion.23
  487.9 0.1 fusion.32
  488.0 0.0 copy-start.1
  488.0 3.4 copy.37
  491.4 2.3 reshape_reshape_squeeze.7
  493.8 2.2 fusion.21
  496.0 0.7 reshape.136
  496.7 0.0 copy-done.1
  (13 shorter events, 0.1 us)
Async XLA Ops:
  7.2 7.4 %copy-start = (bf16[4096,32]{0,1:T(8,128)(2,1)S(1)}, bf16[4096,32]{0,1:T(8,128)(2,1)}, u32[]{:S(2)}) copy-start(bf16[4096,32]{0,1:T(8,128)(2,1)} %param.14) | copy-start | bytes 786436
  7.2 7.4 %copy-start.5 = (f32[4096]{0:T(1024)S(1)}, f32[4096]{0:T(1024)}, u32[]{:S(2)}) copy-start(f32[4096]{0:T(1024)} %param.12) | copy-start | bytes 49156
  7.2 121.1 %all-gather.5.cloned.1.call-start = ((), (), s32[]{:S(2)}) async-start(), calls=%async_computation.5 | async-start | bytes 8912896 | tf_op jit(solution)/shard_map/all_gather | solution.py:54
  8.0 180.9 %all-gather.3.cloned.1.call-start = ((), (), s32[]{:S(2)}) async-start(), calls=%async_computation.4 | async-start | bytes 9437184 | tf_op jit(solution)/shard_map/all_gather | solution.py:68
  10.4 4.2 copy-start.2
  17.2 187.2 %all-to-all-start.2 = ((bf16[8,2,256,32]{2,1,3,0:T(2,128)(2,1)}), bf16[8,2,256,32]{2,1,3,0:T(2,128)(2,1)S(1)}, u32[]{:S(2)}, u32[]{:S(2)}) async-start(bf16[8,2,256,32]{2,1,3,0:T(2,128)(2,1)} %broadcast_in_dim.4), calls=%async_computation.2 | async-start | bytes 524288 | tf_op jit(solution)/shard_map/all_to_all | solution.py:19
  46.7 142.2 %copy-start.7 = (f32[1024]{0:T(1024)S(1)}, f32[1024]{0:T(1024)}, u32[]{:S(2)}) copy-start(f32[1024]{0:T(1024)} %param.15) | copy-start | bytes 12292
  204.4 53.6 %all-to-all-start = ((bf16[8,2,2,256,256]{4,3,2,1,0:T(8,128)(2,1)}), bf16[8,2,2,256,256]{4,3,2,1,0:T(8,128)(2,1)}, u32[]{:S(2)}, u32[]{:S(2)}) async-start(bf16[8,2,2,256,256]{4,3,2,1,0:T(8,128)(2,1)} %fusion.12), calls=%async_computation | async-start | bytes 8388608 | tf_op jit(solution)/shard_map/all_to_all | solution.py:73
  257.9 24.8 %all-to-all-start.3 = ((bf16[1,16,1,256,32]{3,4,2,0,1:T(8,128)(2,1)}), bf16[1,16,1,256,32]{3,4,2,0,1:T(8,128)(2,1)S(1)}, u32[]{:S(2)}, u32[]{:S(2)}) async-start(bf16[1,16,1,256,32]{3,4,2,0,1:T(8,128)(2,1)} %bitcast.21), calls=%async_computation.3 | async-start | bytes 524288 | tf_op jit(solution)/shard_map/all_to_all | solution.py:78
  274.7 19.4 %copy-start.6 = (bf16[1,256]{1,0:T(2,128)(2,1)S(1)}, bf16[1,256]{1,0:T(2,128)(2,1)}, u32[]{:S(2)}) copy-start(bf16[1,256]{1,0:T(2,128)(2,1)} %param.18) | copy-start | bytes 1540
  274.7 20.1 %copy-start.8 = (bf16[1,128]{1,0:T(2,128)(2,1)S(1)}, bf16[1,128]{1,0:T(2,128)(2,1)}, u32[]{:S(2)}) copy-start(bf16[1,128]{1,0:T(2,128)(2,1)} %param.19) | copy-start | bytes 772
  282.7 193.1 %all-to-all-start.1 = ((bf16[2,16,1,256,256]{4,3,0,2,1:T(8,128)(2,1)}), bf16[2,16,1,256,256]{4,3,0,2,1:T(8,128)(2,1)}, u32[]{:S(2)}, u32[]{:S(2)}) async-start(bf16[2,16,1,256,256]{4,3,0,2,1:T(8,128)(2,1)} %copy.31), calls=%async_computation.1 | async-start | bytes 8388608 | tf_op jit(solution)/shard_map/all_to_all | solution.py:77
  295.6 191.9 %copy-start.4 = (bf16[4,8,16,256]{3,1,2,0:T(8,128)(2,1)}, bf16[4,8,16,256]{3,1,2,0:T(8,128)(2,1)S(1)}, u32[]{:S(2)}) copy-start(bf16[4,8,16,256]{3,1,2,0:T(8,128)(2,1)S(1)} %copy.43) | copy-start | bytes 786436
  479.7 1.3 copy-start.3
  488.0 8.7 %copy-start.1 = (bf16[4096,32]{0,1:T(8,128)(2,1)S(1)}, bf16[4096,32]{0,1:T(8,128)(2,1)}, u32[]{:S(2)}) copy-start(bf16[4096,32]{0,1:T(8,128)(2,1)} %param.14) | copy-start | bytes 786436
Sparse Core Ops, SparseCore 0:
  9.8 118.4 all-gather.4
  130.7 58.1 all-gather.2
